TPU v7x, 32 devices: a whole 2x2x4 slice. The times are simulated.
32 devices in a mesh: sp: 8 (over z, x), tp: 4 (over y, core).
Axes of the slice: x: 2, y: 2, z: 4, core: 2. Of those that a mesh axis runs over, the one named last changes fastest.
Arguments:
- probe_vectors: bfloat16 [1024, 2048], P('sp', 'tp'), may hold values from -6 to 6
- address_vectors: bfloat16 [1024, 2048], P('sp', 'tp'), may hold values from -6 to 6
- content_vectors: bfloat16 [1024, 2048], P('sp', 'tp'), may hold values from -6 to 6
- storage_raw_signal: float32 [16, 1024], P('tp', 'sp'), may hold values from -8 to 4
- fade_raw_signal: float32 [16, 1024], P('tp', 'sp'), may hold values from -6 to 6
- channel_fade_exponent: float32 [16], P('tp'), may hold values from -9 to 0
- extra_fade_amount: float32 [16, 1024], P('tp', 'sp'), may hold values from -1 to 0
- sequence_label: int32 [1024], P('sp'), may hold values from 0 to 2, never falling along the last dimension, each value on 1 to 768 neighbouring positions
- exit_valve_raw_signal: bfloat16 [1024, 2048], P('sp', 'tp'), may hold values from -6 to 6
- final_projection_matrix: bfloat16 [2048, 2048], P('tp'), may hold values from -0.125 to 0.125
- incoming_rows_matrix: bfloat16 [1024, 2048], P('sp', 'tp'), may hold values from -48 to 48
- initial_rescale_factor: float32 [2048], P('tp'), may hold values from 0 to 3
- specialist_picks: int32 [1024, 2], P('sp'), may hold values from 0 to 7, all different within a row; in each aligned block of 128 rows (0 to 127, 128 to 255, ...) at most 36 rows name the same one
- picked_specialist_share: bfloat16 [1024, 2], P('sp'), may hold values from 0.29882812 to 1.1953125
- specialist_valve_matrix: bfloat16 [8, 2048, 4096], P('sp', None, 'tp'), may hold values from -0.125 to 0.125
- specialist_raising_matrix: bfloat16 [8, 2048, 4096], P('sp', None, 'tp'), may hold values from -0.125 to 0.125
- specialist_lowering_matrix: bfloat16 [8, 4096, 2048], P('sp', 'tp'), may hold values from -0.09375 to 0.09375
- common_valve_matrix: bfloat16 [2048, 512], P(None, 'tp'), may hold values from -0.125 to 0.125
- common_raising_matrix: bfloat16 [2048, 512], P(None, 'tp'), may hold values from -0.125 to 0.125
- common_lowering_matrix: bfloat16 [512, 2048], P('tp'), may hold values from -0.25 to 0.25
- latter_rescale_factor: float32 [2048], P('tp'), may hold values from 0.1 to 1.9
Outputs:
- result: bfloat16 [1024, 2048], P('sp', 'tp')
Inputs may be any that keep to these rules, and one draw needn't show every extreme that they name: `sequence_label`: document numbers never fall; a document has 1 to 768 positions, one exactly 768. `specialist_picks`: each row names 2 different experts; among the rows of one index of sp no expert is named more than 36 times, a bound that some block reaches.
All inputs are finite; a program needn't handle non-finite values.
Results may differ from a plain program's by a relative error of at most 0.018.
Values may be sent and summed in bfloat16 or wider, within the bound.
A program may use at most 64 MiB of HBM per device.

v0:
```python
import functools

import jax
import jax.numpy as jnp
from jax import lax
from jax.experimental import pallas as pl
from jax.experimental.pallas import tpu as pltpu
from jax.sharding import PartitionSpec as P

DK = 128
DV = 128
BLOCK = 64
DOC_SPAN = 768


HIGH = lax.Precision.HIGH
ALPHA = 2.0**0.25
MESH = pl.DeviceIdType.MESH


def vmem_specs(count):
    return [pl.BlockSpec(memory_space=pltpu.VMEM)] * count


def scan_plan(n, reach):
    hops = [1]
    covered = 1
    if reach > 1 and n > 2:
        hops.append(2)
        covered = 3
        while covered < min(reach, n - 1):
            hops.append(covered)
            covered = 2 * covered
    return hops


def scan_kernel(n, hops, own_ref, label_ref, out_ref, *scratch):
    rounds = len(hops)
    landed, built = scratch[:rounds], scratch[rounds : 2 * rounds]
    send_sem, recv_sem, label_in, label_sem = scratch[2 * rounds :]
    heads = own_ref.shape[1]
    me = lax.axis_index("sp")
    barrier = pltpu.get_barrier_semaphore()
    for hop in range(1, n):
        pl.semaphore_signal(
            barrier, inc=1, device_id={"sp": lax.rem(me + hop, n)}, device_id_type=MESH
        )
    pl.semaphore_wait(barrier, n - 1)

    def dot(left, right):
        return jnp.dot(left, right, preferred_element_type=jnp.float32)

    def copy_of(index):
        last = index == rounds - 1 and index > 1
        source = built[index]
        landing = landed[index]
        if last:
            source, landing = source.at[1], landing.at[1]
        return pltpu.make_async_remote_copy(
            src_ref=source,
            dst_ref=landing,
            send_sem=send_sem.at[index],
            recv_sem=recv_sem.at[index],
            device_id={"sp": lax.rem(me + hops[index], n)},
            device_id_type=MESH,
        )

    note = pltpu.make_async_remote_copy(
        src_ref=label_ref,
        dst_ref=label_in,
        send_sem=label_sem.at[0],
        recv_sem=label_sem.at[1],
        device_id={"sp": lax.rem(me + 1, n)},
        device_id_type=MESH,
    )
    note.start()
    note.wait_recv()
    before, first = label_in[0:1, label_in.shape[1] - 1 :], label_ref[0:1, 0:1]
    joined = ((before == first) & (me > 0)).astype(jnp.float32)
    for h in range(heads):
        built[0][0, h] = (own_ref[0, h] * joined).astype(built[0].dtype)
        built[0][1, h] = own_ref[1, h].astype(built[0].dtype)
    window = None
    for index, hop in enumerate(hops):
        copy = copy_of(index)
        last = index == rounds - 1

        @pl.when(me + hop < n)
        def _():
            copy.start()

        @pl.when(me >= hop)
        def _():
            copy.wait_recv()

        @pl.when(me < hop)
        def _():
            landed[index][...] = jnp.zeros_like(landed[index])

        got = landed[index]
        if index == 0:
            if last:
                out_ref[...] = got[1].astype(jnp.float32) * joined
            else:
                later, target = built[0], built[1]
                for h in range(heads):
                    target[0, h] = dot(later[0, h], got[0, h]).astype(target.dtype)
                    target[1, h] = (
                        dot(later[0, h], got[1, h]) + later[1, h].astype(jnp.float32)
                    ).astype(target.dtype)
            window = got
        else:
            for h in range(heads):
                shift = dot(window[0, h], got[1, h]) + window[1, h].astype(jnp.float32)
                if last:
                    out_ref[h] = shift * joined
                else:
                    target = built[index + 1]
                    target[0, h] = dot(window[0, h], got[0, h]).astype(target.dtype)
                    target[1, h] = shift.astype(target.dtype)
            if not last:
                window = built[index + 1]
    for index, hop in enumerate(hops):

        @pl.when(me + hop < n)
        def _():
            copy_of(index).wait_send()

    note.wait_send()


def entering(summary, labels, reach, cid):
    n = lax.axis_size("sp")
    hops = scan_plan(n, reach)
    block = pltpu.VMEM(summary.shape, jnp.bfloat16)
    return pl.pallas_call(
        functools.partial(scan_kernel, n, hops),
        out_shape=jax.ShapeDtypeStruct(summary.shape[1:], jnp.float32),
        in_specs=vmem_specs(2),
        out_specs=pl.BlockSpec(memory_space=pltpu.VMEM),
        scratch_shapes=[block] * (2 * len(hops))
        + [pltpu.SemaphoreType.DMA((len(hops),)), pltpu.SemaphoreType.DMA((len(hops),))]
        + [pltpu.VMEM(labels.shape, labels.dtype), pltpu.SemaphoreType.DMA((2,))],
        compiler_params=pltpu.CompilerParams(collective_id=cid, has_side_effects=True),
        name="state_scan",
    )(summary, labels)


def unit_rows(array):
    return array * lax.rsqrt(jnp.sum(array * array, -1, keepdims=True) + 1e-06)


def matmul_high(form, left, right):
    return jnp.einsum(form, left, right, precision=HIGH)


def matmul_one(form, left, right):
    return jnp.einsum(
        form,
        left.astype(jnp.bfloat16),
        right.astype(jnp.bfloat16),
        preferred_element_type=jnp.float32,
    )


def row_stats(array):
    lane = lax.broadcasted_iota(jnp.int32, (array.shape[0], 128), 1)
    total = jnp.sum(array, -1, keepdims=True)
    square = jnp.sum(array * array, -1, keepdims=True)
    return jnp.where(lane == 0, total, jnp.where(lane == 1, square, 0.0)).T[:8]


def columns_of(rows):
    return jnp.concatenate([rows] * (128 // rows.shape[0]), 0).T


def layer_kernel(
    ns, nt, cap, pad, heads_ref, wo_ref, rows_ref, gain_ref, last_gain_ref, pick_ref, pick_t_ref,
    info_ref, wv_hbm, wr_hbm, wd_hbm, cv_hbm, cr_hbm, cd_hbm, out_ref,
    wv_ref, wr_ref, wd_ref, cv_ref, cr_ref, cd_ref, weight_sem,
    head_out, head_in, head_yout, head_yin, head_sem,
    stat_own, stat_in, stat_sem,
    sbuf, gathered, infos, sp_sem, info_sem, y_sem, pair_sem,
    inputs, hidden, shared, side, part_out, part_in, part_yout, part_yin, part_sem,
    back_out, back_in, back_sem, returned,
):
    sp, tp = lax.axis_index("sp"), lax.axis_index("tp")
    chips = nt // 2
    chip, core = tp // 2, lax.rem(tp, 2)
    partner = tp + 1 - 2 * core
    width = out_ref.shape[-1]
    loads = [
        pltpu.make_async_copy(source, target, weight_sem.at[i])
        for i, (source, target) in enumerate(
            (
                (cv_hbm, cv_ref),
                (cr_hbm, cr_ref),
                (wv_hbm.at[0], wv_ref),
                (wr_hbm.at[0], wr_ref),
                (cd_hbm, cd_ref),
                (wd_hbm.at[0], wd_ref),
            )
        )
    ]
    for load in loads:
        load.start()
    barrier = pltpu.get_barrier_semaphore()
    for hop in range(1, ns):
        pl.semaphore_signal(
            barrier, inc=1, device_id={"sp": lax.rem(sp + hop, ns)}, device_id_type=MESH
        )
    for hop in range(1, nt):
        pl.semaphore_signal(
            barrier, inc=1, device_id={"tp": lax.rem(tp + hop, nt)}, device_id_type=MESH
        )
    inputs[...] = jnp.zeros_like(inputs)
    returned[...] = jnp.zeros_like(returned)
    pl.semaphore_wait(barrier, ns - 1 + nt - 1)
    waits = []

    def send(source, target, sems, place, where):
        copy = pltpu.make_async_remote_copy(
            src_ref=source,
            dst_ref=target,
            send_sem=sems.at[(0,) + place],
            recv_sem=sems.at[(1,) + place],
            device_id=where,
            device_id_type=MESH,
        )
        copy.start()
        waits.append(copy)
        return copy

    def dot(left, right):
        return jnp.dot(left, right, preferred_element_type=jnp.float32)

    def sum_over_tp(block, put, take, out, landed, yout, yin, sems):
        order = list(range(1, chips)) + [0]
        pairs = {}
        for k in order:
            put(out, k, block(2 * lax.rem(chip + k, chips) + 1 - core))
            pairs[k] = send(out.at[k], landed.at[k], sems, (k,), {"tp": partner})
        across = []
        for k in order:
            there = 2 * lax.rem(chip + k, chips) + core
            value = block(there)
            pairs[k].wait_recv()
            value = value + take(landed, k)
            if k:
                put(yout, k - 1, value)
                across.append(
                    send(yout.at[k - 1], yin.at[k - 1], sems, (chips + k - 1,), {"tp": there})
                )
        for k, copy in enumerate(across):
            copy.wait_recv()
            value = value + take(yin, k)
        return value

    def normed(summed, gain, index):
        stat_own[index] = row_stats(summed)
        copies = []
        for hop in range(1, nt):
            copies.append(
                send(
                    stat_own.at[index],
                    stat_in.at[index, hop - 1],
                    stat_sem,
                    (index, hop - 1),
                    {"tp": lax.rem(tp + hop, nt)},
                )
            )
        total = stat_own[index]
        for hop in range(1, nt):
            copies[hop - 1].wait_recv()
            total = total + stat_in[index, hop - 1]
        total = columns_of(total / (width * nt))
        mean, square = total[:, 0:1], total[:, 1:2]
        return (summed - mean) * lax.rsqrt(square - mean * mean + 1e-05) * gain

    def head_block(t):
        start = pl.multiple_of(t * width, width)
        return dot(heads_ref[...], wo_ref[:, pl.ds(start, width)])

    def put_plain(ref, k, value):
        ref[k] = value.astype(ref.dtype)

    def take_plain(ref, k):
        return ref[k].astype(jnp.float32)

    projected = sum_over_tp(
        head_block, put_plain, take_plain, head_out, head_in, head_yout, head_yin, head_sem
    )
    middle = normed(
        ALPHA * rows_ref[...].astype(jnp.float32) + projected, gain_ref[...], 0
    ).astype(jnp.bfloat16)
    picked = dot(pick_ref[...], middle).astype(jnp.bfloat16)
    for e in range(ns):
        sbuf[e] = picked[e * pad : e * pad + cap]
    arrivals, notes = [], []
    for hop in range(1, ns):
        to = lax.rem(sp + hop, ns)
        notes.append(
            send(info_ref.at[to], infos.at[sp], info_sem, (hop - 1,), {"sp": to})
        )
        arrivals.append(
            send(sbuf.at[to], gathered.at[tp, sp], sp_sem, (hop - 1,), {"sp": to})
        )
    gathered[tp, sp] = sbuf[sp]
    infos[sp] = info_ref[sp]
    forward, across = [], []
    for hop in range(ns):
        source = lax.rem(sp - hop + ns, ns)
        if hop:
            arrivals[hop - 1].wait_recv()
        mine = gathered.at[tp, source]
        for k in range(1, chips):
            across.append(
                (
                    hop,
                    k,
                    send(
                        mine, mine, y_sem, (hop, k - 1),
                        {"tp": 2 * lax.rem(chip + k, chips) + core},
                    ),
                )
            )
        forward.append(send(mine, mine, pair_sem, (hop, 0), {"tp": partner}))
    for hop, k, copy in across:
        copy.wait_recv()
        source = lax.rem(sp - hop + ns, ns)
        theirs = gathered.at[2 * lax.rem(chip - k + chips, chips) + core, source]
        forward.append(send(theirs, theirs, pair_sem, (hop, k), {"tp": partner}))
    for copy in forward + notes:
        copy.wait_recv()
    for j in range(ns):
        for t in range(nt):
            inputs[j * pad : j * pad + cap, t * width : (t + 1) * width] = gathered[t, j]
        note = columns_of(infos[j])[:pad]
        side[j * pad : (j + 1) * pad] = note
    weight_e, shared_e = side[:, 0:1], side[:, 1:2]
    for load in loads[:4]:
        load.wait()
    shared[...] = (
        jax.nn.silu(dot(inputs[...], cv_ref[...])) * dot(inputs[...], cr_ref[...]) * shared_e
    ).astype(jnp.bfloat16)
    units = hidden.shape[1]
    tile = 256 if units % 256 == 0 else 128

    @pl.loop(0, units // tile)
    def _(i):
        cols = pl.ds(pl.multiple_of(i * tile, tile), tile)
        gate = dot(inputs[...], wv_ref[:, cols])
        up = dot(inputs[...], wr_ref[:, cols])
        hidden[:, cols] = (jax.nn.silu(gate) * up * weight_e).astype(jnp.bfloat16)

    for load in loads[4:]:
        load.wait()

    def part_block(t):
        cols = pl.ds(pl.multiple_of(t * width, width), width)
        return dot(hidden[...], wd_ref[:, cols]) + dot(shared[...], cd_ref[:, cols])

    def put_groups(ref, k, value):
        value = value.astype(ref.dtype)
        for j in range(ns):
            ref[k, j] = value[j * pad : j * pad + cap]

    def take_padded(ref, k):
        for j in range(ns):
            returned[j * pad : j * pad + cap] = ref[k, j]
        return returned[...].astype(jnp.float32)

    summed = sum_over_tp(
        part_block, put_groups, take_padded, part_out, part_in, part_yout, part_yin, part_sem
    )
    put_groups(back_out, 0, summed)
    backs = []
    for hop in range(1, ns):
        to = lax.rem(sp + hop, ns)
        backs.append(send(back_out.at[0, to], back_in.at[sp], back_sem, (hop - 1,), {"sp": to}))
    back_in[sp] = back_out[0, sp]
    for copy in backs:
        copy.wait_recv()
    for j in range(ns):
        returned[j * pad : j * pad + cap] = back_in[j]
    mixture = dot(pick_t_ref[...], returned[...])
    result = normed(ALPHA * middle.astype(jnp.float32) + mixture, last_gain_ref[...], 1)
    out_ref[...] = result.astype(out_ref.dtype)
    for copy in waits:
        copy.wait_send()


def layer(heads_out, wo, rows, gain, last_gain, pick, pick_t, info, weights, cap, pad, cid):
    ns, nt = lax.axis_size("sp"), lax.axis_size("tp")
    chips = nt // 2
    tokens, width = rows.shape
    wv, wr, wd, cv, cr, cd = weights
    half, dma = jnp.bfloat16, pltpu.SemaphoreType.DMA
    across = max(chips - 1, 1)

    def vm(*shape, dtype=half):
        return pltpu.VMEM(shape, dtype)

    scratch = [
        vm(*wv.shape[1:]), vm(*wr.shape[1:]), vm(*wd.shape[1:]),
        vm(*cv.shape), vm(*cr.shape), vm(*cd.shape), dma((6,)),
        vm(chips, tokens, width), vm(chips, tokens, width),
        vm(across, tokens, width), vm(across, tokens, width), dma((2, 2 * chips)),
        vm(2, 8, tokens, dtype=jnp.float32), vm(2, nt - 1, 8, tokens, dtype=jnp.float32),
        dma((2, 2, nt - 1)),
        vm(ns, cap, width), vm(nt, ns, cap, width), vm(ns, 8, 128, dtype=jnp.float32),
        dma((2, ns - 1)), dma((2, ns - 1)), dma((2, ns, across)), dma((2, ns, chips)),
        vm(ns * pad, width * nt), vm(ns * pad, wv.shape[2]), vm(ns * pad, cv.shape[1]),
        vm(ns * pad, 128, dtype=jnp.float32),
        vm(chips, ns, cap, width), vm(chips, ns, cap, width),
        vm(across, ns, cap, width), vm(across, ns, cap, width), dma((2, 2 * chips)),
        vm(1, ns, cap, width), vm(ns, cap, width), dma((2, ns - 1)), vm(ns * pad, width),
    ]
    return pl.pallas_call(
        functools.partial(layer_kernel, ns, nt, cap, pad),
        out_shape=jax.ShapeDtypeStruct((tokens, width), half),
        in_specs=vmem_specs(8) + [pl.BlockSpec(memory_space=pl.ANY)] * 6,
        out_specs=pl.BlockSpec(memory_space=pltpu.VMEM),
        scratch_shapes=scratch,
        compiler_params=pltpu.CompilerParams(
            collective_id=cid, has_side_effects=True, vmem_limit_bytes=60 * 2**20
        ),
        name="layer",
    )(heads_out, wo, rows, gain, last_gain, pick, pick_t, info, *weights)


def block_pass(query_unit, key_unit, write_gate, decay_logarithm, segment, values_in, initial):
    heads_here, blocks, block_len, key_depth = query_unit.shape
    cumulative = jnp.cumsum(decay_logarithm, -1)
    before = jnp.concatenate([segment[:1, 0], segment[:-1, -1]])
    carried = (segment == before[:, None]).astype(jnp.float32)
    same_doc = segment[:, :, None] == segment[:, None, :]
    offsets = jnp.arange(block_len)
    lower_tri = offsets[:, None] >= offsets[None, :]
    strict = offsets[:, None] > offsets[None, :]
    log_gap = cumulative[..., :, None] - cumulative[..., None, :]
    reach_mask = jnp.where(lower_tri & same_doc, jnp.exp(jnp.where(lower_tri, log_gap, 0.0)), 0.0)
    weighted_keys = key_unit * write_gate[..., None]
    coupling = jnp.where(
        strict, matmul_high("hncd,hnsd->hncs", weighted_keys, key_unit) * reach_mask, 0.0
    )
    identity_block = jnp.eye(block_len, dtype=jnp.float32)
    inverse = identity_block - coupling
    nil_power = coupling
    for squaring in range(block_len.bit_length() - 2):
        nil_power = matmul_high("hncs,hnst->hnct", nil_power, nil_power)
        inverse = matmul_high("hncs,hnst->hnct", inverse, identity_block + nil_power)
    growth = jnp.exp(cumulative) * carried
    update = matmul_one("hncs,hnse->hnce", inverse, values_in * write_gate[..., None])
    correction = matmul_one("hncs,hnsd->hncd", inverse, weighted_keys * growth[..., None])
    final_growth = jnp.exp(cumulative[..., -1]) * (segment[:, -1] == before).astype(jnp.float32)
    tail_decay = jnp.exp(cumulative[..., -1:] - cumulative) * (segment == segment[:, -1:]).astype(
        jnp.float32
    )
    tail_keys = key_unit * tail_decay[..., None]
    query_grown = query_unit * growth[..., None]
    local_scores = matmul_one("hncd,hnsd->hncs", query_unit, key_unit) * reach_mask

    def advance(carry_state, inputs):
        grown_query, block_corr, block_update, block_keys, block_scores, block_fade = inputs
        fresh_values = block_update - matmul_one("hcd,hde->hce", block_corr, carry_state)
        next_state = carry_state * block_fade[:, None, None] + matmul_one(
            "hcd,hce->hde", block_keys, fresh_values
        )
        block_out = matmul_one("hcd,hde->hce", grown_query, carry_state) + matmul_one(
            "hcs,hse->hce", block_scores, fresh_values
        )
        return (next_state, block_out)

    inputs = tuple(
        (
            jnp.moveaxis(array, 1, 0)
            for array in (query_grown, correction, update, tail_keys, local_scores, final_growth)
        )
    )
    final_state, outputs = lax.scan(advance, initial, inputs)
    outputs = jnp.moveaxis(outputs, 0, 1).reshape(heads_here, blocks * block_len, -1)
    return (final_state, outputs)


def shards(
    probe_vectors,
    address_vectors,
    content_vectors,
    storage_raw_signal,
    fade_raw_signal,
    channel_fade_exponent,
    extra_fade_amount,
    sequence_label,
    exit_valve_raw_signal,
    final_projection_matrix,
    incoming_rows_matrix,
    initial_rescale_factor,
    specialist_picks,
    picked_specialist_share,
    specialist_valve_matrix,
    specialist_raising_matrix,
    specialist_lowering_matrix,
    common_valve_matrix,
    common_raising_matrix,
    common_lowering_matrix,
    latter_rescale_factor,
):
    tokens_here = probe_vectors.shape[0]
    heads_here = storage_raw_signal.shape[0]
    blocks = tokens_here // BLOCK

    def split_heads(array, width):
        moved = jnp.transpose(
            array.astype(jnp.float32).reshape(tokens_here, heads_here, width), (1, 0, 2)
        )
        return moved.reshape(heads_here, blocks, BLOCK, width)

    query_unit = unit_rows(split_heads(probe_vectors, DK)) * DK ** (-0.5)
    key_unit = unit_rows(split_heads(address_vectors, DK))
    value_rows = split_heads(content_vectors, DV)
    write_gate = jax.nn.sigmoid(storage_raw_signal).reshape(heads_here, blocks, BLOCK)
    decay_logarithm = (
        extra_fade_amount
        - jnp.exp(channel_fade_exponent)[:, None] * jax.nn.softplus(fade_raw_signal)
    ).reshape(heads_here, blocks, BLOCK)
    segment = sequence_label.astype(jnp.float32).reshape(blocks, BLOCK)
    extended = jnp.concatenate(
        [value_rows, jnp.zeros((heads_here, blocks, BLOCK, DK), jnp.float32)], -1
    )
    identity_state = jnp.broadcast_to(jnp.eye(DK, dtype=jnp.float32), (heads_here, DK, DK))
    start_state = jnp.concatenate(
        [jnp.zeros((heads_here, DK, DV), jnp.float32), identity_state], -1
    )
    summary, local_out = block_pass(
        query_unit, key_unit, write_gate, decay_logarithm, segment, extended, start_state
    )
    reach = -(-(DOC_SPAN - 1) // tokens_here)
    own = jnp.stack([summary[..., DV:], summary[..., :DV]])
    incoming = entering(own, sequence_label[None, :], reach, 1)
    memory_layer_result = local_out[..., :DV] + matmul_one(
        "hcd,hde->hce", local_out[..., DV:], incoming
    )
    scaled = memory_layer_result * lax.rsqrt(
        jnp.mean(memory_layer_result * memory_layer_result, -1, keepdims=True) + 1e-06
    )
    token_major = jnp.transpose(scaled, (1, 0, 2)).reshape(tokens_here, heads_here * DV)
    heads_out = (token_major * jax.nn.silu(exit_valve_raw_signal.astype(jnp.float32))).astype(
        jnp.bfloat16
    )
    top = specialist_picks.shape[1]
    local_experts = specialist_valve_matrix.shape[0]
    experts_all = local_experts * lax.axis_size("sp")
    capacity = max(2, 9 * tokens_here * top // (8 * experts_all))
    picks = tokens_here * top
    flat_routes = specialist_picks.reshape(picks)
    one_hot = (flat_routes[:, None] == jnp.arange(experts_all, dtype=jnp.int32)[None, :]).astype(
        jnp.int32
    )
    rank_in = jnp.sum(jnp.cumsum(one_hot, 0) * one_hot, 1) - 1
    pad = -(-capacity // 16) * 16
    slot_table = (flat_routes * pad + rank_in).reshape(tokens_here, top)
    order = jnp.arange(experts_all * pad, dtype=jnp.int32)
    matches = [order[:, None] == slot_table[None, :, j] for j in range(top)]
    pick = functools.reduce(jnp.logical_or, matches).astype(jnp.bfloat16)
    turned = [order[None, :] == slot_table[:, j, None] for j in range(top)]
    pick_t = functools.reduce(jnp.logical_or, turned).astype(jnp.bfloat16)
    slot_weight = sum(
        jnp.sum(jnp.where(turned[j], picked_specialist_share[:, j, None].astype(jnp.float32), 0.0), 0)
        for j in range(top)
    )
    slot_shared = jnp.any(turned[0], 0).astype(jnp.float32)
    info = jnp.stack([slot_weight, slot_shared]).reshape(2, experts_all, pad)
    info = jnp.pad(jnp.moveaxis(info, 0, 1), ((0, 0), (0, 6), (0, 128 - pad)))
    return layer(
        heads_out,
        final_projection_matrix,
        incoming_rows_matrix,
        initial_rescale_factor[None, :],
        latter_rescale_factor[None, :],
        pick,
        pick_t,
        info,
        (
            specialist_valve_matrix,
            specialist_raising_matrix,
            specialist_lowering_matrix,
            common_valve_matrix,
            common_raising_matrix,
            common_lowering_matrix,
        ),
        capacity,
        pad,
        2,
    )


def solution(mesh):
    placed = (
        P("sp", "tp"),
        P("sp", "tp"),
        P("sp", "tp"),
        P("tp", "sp"),
        P("tp", "sp"),
        P("tp"),
        P("tp", "sp"),
        P("sp"),
        P("sp", "tp"),
        P("tp", None),
        P("sp", "tp"),
        P("tp"),
        P("sp", None),
        P("sp", None),
        P("sp", None, "tp"),
        P("sp", None, "tp"),
        P("sp", "tp", None),
        P(None, "tp"),
        P(None, "tp"),
        P("tp", None),
        P("tp"),
    )
    return jax.shard_map(
        shards, mesh=mesh, in_specs=placed, out_specs=P("sp", "tp"), check_vma=False
    )
```

profile of v0, /device:TPU:0, one launch (start us, length us, event | category | flops | bytes accessed | tf_op | source)
XLA Modules:
  0.0 109.7 jit_solution(9551150815848308525)
XLA Ops:
  0.0 0.7 convert_element_type.135
  0.9 1.0 copy.80
  2.2 0.7 exp.37
  2.8 0.8 fusion.64
  3.7 0.9 reduce_window_sum.26
  4.6 0.7 add_divide_fusion
  5.4 0.5 fusion.19
  6.0 0.3 fusion.68
  6.3 0.3 fusion.35
  6.5 0.3 fusion.69
  7.1 0.3 fusion.70
  7.6 0.3 fusion.71
  8.1 0.3 convolution_add_fusion.3
  8.6 0.7 fusion.67
  9.5 1.4 %compare_convert_fusion.2 = (f32[2]{0:T(128)S(1)}, f32[2]{0:T(128)S(1)}) fusion(f32[2]{0:T(128)S(1)} %slice_reduce_fusion.1, f32[1]{0:T(128)} %bitcast.9, f32[1]{0:T(128)} %bitcast.8), kind=kLoop, calls=%fused_computation.119 | loop fusion | flops 6 | bytes 32 | tf_op jit(solution)/shard_map/convert_element_type | solution.py:456
  11.3 0.4 convolution_bitcast_fusion.2
  11.8 0.3 convolution_bitcast_fusion
  12.6 0.3 multiply_bitcast_fusion.1
  12.9 0.3 fusion.20
  13.4 1.9 %while.12 = (s32[]{:T(128)}, f32[4,128,256]{2,1,0:T(8,128)S(1)}, f32[2,4,64,256]{3,2,1,0:T(8,128)S(1)}, f32[2,4]{1,0:T(2,128)S(1)}, bf16[2,4,64,128]{3,2,0,1:T(8...) while((s32[]{:T(128)}, f32[4,128,256]{2,1,0:T(8,128)S(1)}, ...), condition=%wide.region_4.5_spmd, body=%wide.region_3.4_spmd.sunk | while | flops 59441152 | bytes 3803793 | solution.py:481
  14.0 0.4 convolution_add_fusion.5
  14.9 0.4 convolution_add_fusion.5
  15.4 0.8 pad_maximum_fusion.own_ref
  16.2 17.8 %state_scan.1 = f32[4,128,128]{2,1,0:T(8,128)} custom-call(f32[2,4,128,128]{3,2,1,0:T(8,128)} %pad_maximum_fusion.own_ref, s32[1,128]{1,0:T(1,128)} %bitcast.175), custom_call_target="tpu_custom_call" | custom-call | tf_op jit(solution)/shard_map/state_scan/pallas_call | solution.py:136
  34.1 1.2 %multiply_reduce_fusion = (f32[4,128]{1,0:T(4,128)S(1)}, f32[4,128,128]{2,1,0:T(8,128)S(1)}) fusion(f32[4,128,128]{2,1,0:T(8,128)} %state_scan.1, f32[4,128,256]{2,1,0:T(8,128)S(1)} %bitcast.159), kind=kOutput, calls=%fused_computation.47 | convolution fusion | flops 17104384 | bytes 1050624 | tf_op jit(solution)/shard_map/hcd,hde->hce/dot_general | solution.py:158
  35.3 0.8 fusion.38.heads_ref
  36.4 0.6 reduce-window.6
  38.0 0.8 fusion.41
  38.9 0.6 pad.7.info_ref
  39.5 0.7 fusion.44.pick_ref
  40.2 68.0 %layer.1 = bf16[128,512]{1,0:T(8,128)(2,1)} custom-call(bf16[128,512]{1,0:T(8,128)(2,1)} %fusion.38.heads_ref, bf16[512,2048]{1,0:T(8,128)(2,1)} %wo_ref.1, bf16[128,512]{1,0:T(8,128)(2,1)} %rows_ref.1, f32[1,512]{1,0:T(1,128)} %bitcast.173, f32[1,512]{1,0:T(1,128)} %bitcast.174, bf16[384,128]{1,0:T(8,128)(2,1)} %fusion.44.pick_ref, ...), custom_call_target="tpu_custom_call" | custom-call | tf_op jit(solution)/shard_map/layer/pallas_call | solution.py:419
  108.1 1.6 %copy.120 = bf16[128,512]{1,0:T(8,128)(2,1)} copy(bf16[128,512]{1,0:T(8,128)(2,1)} %layer.1) | data formatting | bytes 262144
  (75 shorter events, 5.3 us)
Async XLA Ops:
  6.0 5.8 %copy-start = (bf16[128,512]{1,0:T(8,128)(2,1)S(1)}, bf16[128,512]{1,0:T(8,128)(2,1)}, u32[]{:S(2)}) copy-start(bf16[128,512]{1,0:T(8,128)(2,1)} %param.25) | copy-start | bytes 393220
  6.5 5.6 %copy-start.1 = (bf16[128,512]{1,0:T(8,128)(2,1)S(1)}, bf16[128,512]{1,0:T(8,128)(2,1)}, u32[]{:S(2)}) copy-start(bf16[128,512]{1,0:T(8,128)(2,1)} %param.23) | copy-start | bytes 393220
  15.3 20.0 %copy-start.2 = (bf16[128,512]{1,0:T(8,128)(2,1)S(1)}, bf16[128,512]{1,0:T(8,128)(2,1)}, u32[]{:S(2)}) copy-start(bf16[128,512]{1,0:T(8,128)(2,1)} %param.31) | copy-start | bytes 393220
  15.3 20.8 %copy-start.3 = (s32[128,2]{0,1:T(2,128)S(1)}, s32[128,2]{0,1:T(2,128)}, u32[]{:S(2)}) copy-start(s32[128,2]{0,1:T(2,128)} %param.35) | copy-start | bytes 3076
  15.3 22.4 %copy-start.4 = (bf16[128,2]{0,1:T(2,128)(2,1)S(1)}, bf16[128,2]{0,1:T(2,128)(2,1)}, u32[]{:S(2)}) copy-start(bf16[128,2]{0,1:T(2,128)(2,1)} %param.36) | copy-start | bytes 1540
where the time goes:
time: 110 us
  Pallas kernels  85.8 us (78%)
  other arithmetic  9.26 us (8%)
  matrix products  7.11 us (6%)
  local copies, waits for them, and re-layouts  7.01 us (6%)
    pallas_call x1, Pallas kernels, layer(): pl.pallas_call(functools.partial(layer_kernel, ns, nt, cap, pad), out_sha...  68 us
    pallas_call x1, Pallas kernels, entering(): pl.pallas_call(functools.partial(scan_kernel, n, hops), out_shape=jax.Sha...  17.8 us
    dot_general x12, matrix products, matmul_one(): jnp.einsum(form, left.astype(jnp.bfloat16), right.astype(jnp.bfloat16), p...  4.03 us
    dot_general x11, matrix products, matmul_high(): return jnp.einsum(form, left, right, precision=HIGH)  3.08 us
    unnamed x14, local copies, waits for them, and re-layouts  2.85 us

commit v1 on v0

v1 whole, which is shorter than its diff:
```python
import functools
from types import SimpleNamespace

import jax
import jax.numpy as jnp
from jax import lax
from jax.experimental import pallas as pl
from jax.experimental.pallas import tpu as pltpu
from jax.sharding import PartitionSpec as P

DK = 128
DV = 128
DOC_SPAN = 768
GROUP = 4

ALPHA = 2.0**0.25
MESH = pl.DeviceIdType.MESH
F32, BF16 = jnp.float32, jnp.bfloat16


def scan_plan(n, reach):
    hops = [1]
    covered = 1
    if reach > 1 and n > 2:
        hops.append(2)
        covered = 3
        while covered < min(reach, n - 1):
            hops.append(covered)
            covered = 2 * covered
    return hops


def hop_order(n):
    order = [0]
    for near in range(1, n // 2 + 1):
        order.append(near)
        if n - near != near:
            order.append(n - near)
    return order


def dot(left, right):
    return jnp.dot(left, right, preferred_element_type=F32)


def dot_nt(left, right):
    return lax.dot_general(left, right, (((1,), (1,)), ((), ())), preferred_element_type=F32)


def dot_tn(left, right):
    return lax.dot_general(left, right, (((0,), (0,)), ((), ())), preferred_element_type=F32)


def iota(shape, dim):
    return lax.broadcasted_iota(jnp.int32, shape, dim)


def row_stats(array):
    lane = iota((array.shape[0], 128), 1)
    total = jnp.sum(array, -1, keepdims=True)
    square = jnp.sum(array * array, -1, keepdims=True)
    return jnp.where(lane == 0, total, jnp.where(lane == 1, square, 0.0)).T[:8]


def columns_of(rows):
    return jnp.concatenate([rows] * (128 // rows.shape[0]), 0).T


def whole_kernel(plan, *refs):
    r = SimpleNamespace(**dict(zip(plan.names, refs)))
    ns, nt, cap, pad = plan.ns, plan.nt, plan.cap, plan.pad
    size, held, hops = plan.size, plan.held, plan.hops
    order = hop_order(ns)
    groups_all = ns // size
    sp, tp = lax.axis_index("sp"), lax.axis_index("tp")
    chips = nt // 2
    chip, core = tp // 2, lax.rem(tp, 2)
    partner = tp + 1 - 2 * core
    member, group = lax.rem(sp, size), sp // size
    first = group * size
    out_ref = r.out
    tokens, width = out_ref.shape
    heads = r.storage.shape[0]
    span = held * DK
    units, narrow = r.wv_hbm.shape[2], r.cv_hbm.shape[1]
    joint = narrow % 128 == 0
    experts = ns

    hid_w = r.wd
    pairs = [
        (r.wo_hbm, r.wo),
        (r.wv_hbm.at[0], r.wv),
        (r.wr_hbm.at[0], r.wr),
    ]
    if joint:
        pairs += [
            (r.cv_hbm, r.cvr.at[:, :narrow]),
            (r.cr_hbm, r.cvr.at[:, narrow:]),
        ]
    else:
        pairs += [(r.cv_hbm, r.cvr.at[0]), (r.cr_hbm, r.cvr.at[1])]
    pairs += [(r.wd_hbm.at[0], hid_w.at[:units]), (r.cd_hbm, hid_w.at[units:])]
    loads = [
        pltpu.make_async_copy(source, target, r.weight_sem.at[i])
        for i, (source, target) in enumerate(pairs)
    ]
    barrier = pltpu.get_barrier_semaphore()
    for hop in range(1, ns):
        pl.semaphore_signal(
            barrier, inc=1, device_id={"sp": lax.rem(sp + hop, ns)}, device_id_type=MESH
        )
    for hop in range(1, nt):
        pl.semaphore_signal(
            barrier, inc=1, device_id={"tp": lax.rem(tp + hop, nt)}, device_id_type=MESH
        )
    for load in loads:
        load.start()

    row, col = iota((tokens, tokens), 0), iota((tokens, tokens), 1)
    upper = (row <= col).astype(BF16)
    rate = jnp.exp(r.fade_exp[...])
    eye_h = iota((heads, heads), 0) == iota((heads, heads), 1)
    rate = jnp.sum(jnp.where(eye_h, rate, 0.0), 1, keepdims=True)
    decay = r.extra[...] - rate * jnp.log(1.0 + jnp.exp(r.fade[...]))
    write = 1.0 / (1.0 + jnp.exp(-r.storage[...]))
    high = decay.astype(BF16)
    rest = decay - high.astype(F32)
    middle_part = rest.astype(BF16)
    low = (rest - middle_part.astype(F32)).astype(BF16)
    cumulative = dot(high, upper) + dot(middle_part, upper) + dot(low, upper)
    label = r.label[...].astype(F32)
    slot = iota((8, tokens), 0)
    scal_out, scal_in = r.scal_out, r.scal_in
    for h in range(heads):
        tile = jnp.where(slot == 0, write[h : h + 1], 0.0)
        tile = jnp.where(slot == 1, cumulative[h : h + 1], tile)
        scal_out[h] = jnp.where(slot == 2, label, tile)
    r.gain_out[...] = jnp.broadcast_to(r.gain[...], r.gain_out.shape)
    pl.semaphore_wait(barrier, ns - 1 + nt - 1)
    waits = []

    def send(source, target, sems, place, where):
        copy = pltpu.make_async_remote_copy(
            src_ref=source,
            dst_ref=target,
            send_sem=sems.at[(0,) + place],
            recv_sem=sems.at[(1,) + place],
            device_id=where,
            device_id_type=MESH,
        )
        copy.start()
        waits.append(copy)
        return copy

    def part_of(ref, which):
        return ref.at[:, pl.ds(pl.multiple_of(which * span, 128), span)]

    swaps = {}
    for index, name in enumerate(("scal", "keys", "values", "queries", "gate")):
        for p in range(1, size):
            other = lax.rem(member + p, size)
            if name == "scal":
                source, target = scal_out.at[pl.ds(other * held, held)], scal_in.at[member]
            else:
                source, target = part_of(getattr(r, name), other), getattr(r, name + "_in").at[member]
            swaps[name, p] = send(
                source, target, r.swap_sem, (index, p - 1), {"sp": first + other}
            )
    gain_in = r.gain_in
    gain_copies = [
        send(
            r.gain_out, gain_in.at[tp], r.gain_sem, (hop - 1,), {"tp": lax.rem(tp + hop, nt)}
        )
        for hop in range(1, nt)
    ]
    gain_in[tp] = r.gain_out[...]
    for h in range(held):
        scal_in[member, h] = scal_out[member * held + h]
    for name in ("keys", "values", "queries", "gate"):
        getattr(r, name + "_in")[member] = part_of(getattr(r, name), member)[...]

    r.inputs[...] = jnp.zeros_like(r.inputs)
    r.returned[...] = jnp.zeros_like(r.returned)

    pick_a = r.picks[:, 0:1].astype(F32)
    pick_b = r.picks[:, 1:2].astype(F32)
    share = r.share[...].astype(F32)
    lane = iota((tokens, 128), 1)
    lane_f = lane.astype(F32)
    member_of = ((pick_a == lane_f) | (pick_b == lane_f)).astype(F32)
    strict_low = (row > col).astype(BF16)
    ranks = dot(strict_low, member_of.astype(BF16))
    coded = ((ranks + 1.0) * member_of).astype(BF16)
    slots = experts * pad
    owner = iota((128, slots), 0)
    place = iota((128, slots), 1)
    spread = ((place >= owner * pad) & (place < owner * pad + pad)).astype(BF16)
    column = iota((8, slots), 1).astype(F32)
    expert_of = jnp.floor((column + 0.5) * (1.0 / pad))
    local = column - expert_of * pad + 1.0
    pick_t = (dot(coded, spread) == local[0:1]).astype(F32)
    r.pick_t[...] = pick_t.astype(BF16)
    r.pick[...] = pick_t.T.astype(BF16)
    facts = jnp.where(lane == 0, pick_a, 0.0)
    facts = jnp.where(lane == 1, share[:, 0:1], facts)
    facts = jnp.where(lane == 2, share[:, 1:2], facts)
    facts = jnp.where(lane == 3, 1.0, facts).T[:8].astype(BF16)
    facts = dot(facts, pick_t.astype(BF16))
    leads = facts[0:1] == expert_of[0:1]
    slot_weight = jnp.where(leads, facts[1:2], facts[2:3])
    slot_shared = jnp.where(leads, facts[3:4], 0.0)
    side_rows = jnp.where(iota((8, slots), 0) == 0, slot_weight, slot_shared)
    r.info[...] = jnp.zeros_like(r.info)
    for e in range(experts):
        r.info[e, :, 0:pad] = side_rows[:, e * pad : (e + 1) * pad]

    same = row == col
    inverse_ref, decay_ref, norm_ref = r.inverse, r.decay, r.norm

    def invert(blocks):
        coupled, inverse = [], []
        for b, h in blocks:
            keys = r.keys_in[b, :, h * DK : (h + 1) * DK]
            gram = dot_nt(keys, keys)
            tile = scal_in[b, h]
            columns = columns_of(tile)
            diagonal = jnp.where(same, gram, 0.0)
            norm_row = lax.rsqrt(jnp.sum(diagonal, 0, keepdims=True) + 1e-06)
            norm_col = lax.rsqrt(jnp.sum(diagonal, 1, keepdims=True) + 1e-06)
            gap = jnp.where(row >= col, columns[:, 1:2] - tile[1:2], 0.0)
            reach = jnp.where(
                (row >= col) & (columns[:, 2:3] == tile[2:3]), jnp.exp(gap), 0.0
            )
            decay_ref[b, h] = reach
            norm_ref[b, h] = jnp.broadcast_to(norm_row, (8, tokens))
            full = gram * (columns[:, 0:1] * norm_col) * norm_row * reach
            coupled.append(jnp.where(row > col, full, 0.0))
        step = 1
        while step < tokens:
            below = (row // step == col // step + 1) & (lax.rem(row // step, 2) == 1)
            picked = [jnp.where(below, one, 0.0) for one in coupled]
            if step == 1:
                inverse = [same.astype(F32) - one for one in picked]
            else:
                short = [one.astype(BF16) for one in inverse]
                right = [dot(a.astype(BF16), b) for a, b in zip(picked, short)]
                inverse = [
                    one - dot(a, b.astype(BF16)) for one, a, b in zip(inverse, short, right)
                ]
            step = 2 * step
        for (b, h), one in zip(blocks, inverse):
            inverse_ref[b, h] = one

    invert([(member, h) for h in range(held)])
    for name in ("scal", "keys"):
        for p in range(1, size):
            swaps[name, p].wait_recv()
    if size > 1:
        invert(
            [(lax.rem(member - p + size, size), h) for p in range(1, size) for h in range(held)]
        )
    for p in range(1, size):
        swaps["values", p].wait_recv()
    pieces = [(b, h) for b in range(size) for h in range(held)]
    facts_of, updates, steps = {}, {}, {}
    for b, h in pieces:
        tile = scal_in[b, h]
        norm_row = norm_ref[b, h][0:1]
        tile = jnp.where(slot == 3, norm_row, tile)
        columns = columns_of(tile)
        before = scal_in[b - 1, h][2:3, tokens - 1 :] if b else tile[2:3, 0:1]
        last_label, last_sum = tile[2:3, tokens - 1 :], tile[1:2, tokens - 1 :]
        growth_row = jnp.exp(tile[1:2]) * (tile[2:3] == before).astype(F32)
        growth_col = jnp.exp(columns[:, 1:2]) * (columns[:, 2:3] == before).astype(F32)
        tail = jnp.exp(last_sum - columns[:, 1:2]) * (columns[:, 2:3] == last_label).astype(F32)
        fade = jnp.exp(last_sum) * (last_label == before).astype(F32)
        inverse = inverse_ref[b, h]
        keys = r.keys_in[b, :, h * DK : (h + 1) * DK]
        values = r.values_in[b, :, h * DV : (h + 1) * DV]
        update = dot((inverse * tile[0:1]).astype(BF16), values)
        correct = dot((inverse * (tile[0:1] * norm_row * growth_row)).astype(BF16), keys)
        both = jnp.concatenate([update, correct], 1)
        updates[b, h] = both.astype(BF16)
        made = dot_tn(keys, (both * (tail * columns[:, 3:4])).astype(BF16))
        steps[b, h] = (made[:, :DV], made[:, DV:], fade)
        facts_of[b, h] = (growth_col, norm_row)
    built, landed = r.built, r.landed
    rounds = len(hops)
    entry = {}
    summary = {}
    for h in range(held):
        add, erase, fade = steps[0, h]
        carry = jnp.concatenate([jnp.where(same, fade, 0.0) - erase, add], 1)
        for b in range(1, size):
            entry[b, h] = carry.astype(BF16)
            add, erase, fade = steps[b, h]
            carry = fade * carry - dot(erase.astype(BF16), entry[b, h])
            carry = jnp.concatenate([carry[:, :DK], carry[:, DK:] + add], 1)
        summary[h] = carry

    def copy_to_group(source, target, sems, hop):
        return pltpu.make_async_remote_copy(
            src_ref=source,
            dst_ref=target,
            send_sem=sems[0],
            recv_sem=sems[1],
            device_id={"sp": lax.rem(sp + hop * size, ns)},
            device_id_type=MESH,
        )

    def scan_copy(index):
        last = index == rounds - 1
        source, target = built.at[index], landed.at[index]
        if last:
            source, target = source.at[1], target.at[1]
        sems = r.scan_sem.at[0, index], r.scan_sem.at[1, index]
        return copy_to_group(source, target, sems, hops[index])

    note = None
    if groups_all > 1:
        note = copy_to_group(
            scal_in.at[size - 1, 0],
            r.label_note,
            (r.note_sem.at[0], r.note_sem.at[1]),
            1,
        )
        note.start()
        for h in range(held):
            built[0, 1, h] = summary[h][:, DK:].astype(BF16)
    single = rounds == 1
    if groups_all > 1 and single:

        @pl.when(group + hops[0] < groups_all)
        def _():
            scan_copy(0).start()

    for p in range(1, size):
        swaps["queries", p].wait_recv()
    for b, h in pieces:
        growth_col, norm_row = facts_of[b, h]
        keys = r.keys_in[b, :, h * DK : (h + 1) * DK]
        queries = r.queries_in[b, :, h * DK : (h + 1) * DK]
        wide = queries.astype(F32)
        scale = lax.rsqrt(jnp.sum(wide * wide, 1, keepdims=True) + 1e-06) * DK ** (-0.5)
        scores = (dot_nt(queries, keys) * scale * norm_row * decay_ref[b, h]).astype(BF16)
        seen = dot(scores, updates[b, h])
        grown = wide * (scale * growth_col) - seen[:, DV:]
        rows_here = pl.ds(b * tokens, tokens)
        if b:
            carried = dot(grown.astype(BF16), entry[b, h])
            r.reader[h, rows_here] = carried[:, :DK].astype(BF16)
            r.partial[h, rows_here] = seen[:, :DV] + carried[:, DK:]
        else:
            r.reader[h, rows_here] = grown.astype(BF16)
            r.partial[h, rows_here] = seen[:, :DV]
    incoming = None
    if groups_all > 1:
        note.wait_recv()
        joined = (r.label_note[2:3, tokens - 1 :] == scal_in[0, 0][2:3, 0:1]) & (group > 0)
        joined = joined.astype(F32)
        window = None
        if not single:
            for h in range(held):
                built[0, 0, h] = (summary[h][:, :DK] * joined).astype(BF16)
        for index, hop in enumerate(hops):
            last = index == rounds - 1
            if not single:

                @pl.when(group + hop < groups_all)
                def _():
                    scan_copy(index).start()

            @pl.when(group >= hop)
            def _():
                scan_copy(index).wait_recv()

            @pl.when(group < hop)
            def _():
                landed[index] = jnp.zeros_like(landed[index])

            got = landed.at[index]
            if index == 0:
                if last:
                    incoming = [got[1, h].astype(F32) * joined for h in range(held)]
                else:
                    for h in range(held):
                        built[1, 0, h] = dot(built[0, 0, h], got[0, h]).astype(BF16)
                        built[1, 1, h] = (
                            dot(built[0, 0, h], got[1, h]) + built[0, 1, h].astype(F32)
                        ).astype(BF16)
                window = got
            else:
                shifts = [
                    dot(window[0, h], got[1, h]) + window[1, h].astype(F32) for h in range(held)
                ]
                if last:
                    incoming = [one * joined for one in shifts]
                else:
                    for h in range(held):
                        built[index + 1, 0, h] = dot(window[0, h], got[0, h]).astype(BF16)
                        built[index + 1, 1, h] = shifts[h].astype(BF16)
                    window = built.at[index + 1]
    for p in range(1, size):
        swaps["gate", p].wait_recv()
    for h in range(held):
        mixed = r.partial[h]
        if incoming is not None:
            mixed = mixed + dot(r.reader[h], incoming[h].astype(BF16))
        mixed = mixed * lax.rsqrt(jnp.mean(mixed * mixed, -1, keepdims=True) + 1e-06)
        for b in range(size):
            gate = r.gate_in[b, :, h * DV : (h + 1) * DV].astype(F32)
            here = mixed[b * tokens : (b + 1) * tokens] * (gate / (1.0 + jnp.exp(-gate)))
            r.mixed[b, :, h * DV : (h + 1) * DV] = here.astype(BF16)
    gives = []
    for p in range(1, size):
        other = lax.rem(member + p, size)
        gives.append(
            send(
                r.mixed.at[other],
                part_of(r.heads, member),
                r.give_sem,
                (p - 1,),
                {"sp": first + other},
            )
        )
    part_of(r.heads, member)[...] = r.mixed[member]
    for copy in gives:
        copy.wait_recv()
    loads[0].wait()

    def head_block(t):
        start = pl.multiple_of(t * width, width)
        return dot(r.heads[...], r.wo[:, pl.ds(start, width)])

    far_first = list(range(1, chips)) + [0]
    head_pairs, head_across = {}, []
    for k in far_first:
        r.head_out[k] = head_block(2 * lax.rem(chip + k, chips) + 1 - core).astype(BF16)
        head_pairs[k] = send(
            r.head_out.at[k], r.head_in.at[k], r.head_sem, (k,), {"tp": partner}
        )
    for k in far_first:
        there = 2 * lax.rem(chip + k, chips) + core
        value = head_block(there)
        head_pairs[k].wait_recv()
        value = value + r.head_in[k].astype(F32)
        if k:
            r.head_yout[k - 1] = value.astype(BF16)
            head_across.append(
                send(
                    r.head_yout.at[k - 1],
                    r.head_yin.at[k - 1],
                    r.head_sem,
                    (chips + k - 1,),
                    {"tp": there},
                )
            )
    projected = value + ALPHA * r.rows[...].astype(F32)
    for k, copy in enumerate(head_across):
        copy.wait_recv()
        projected = projected + r.head_yin[k].astype(F32)

    picked = dot(r.pick[...], projected.astype(BF16)).astype(BF16)
    sbuf, gathered, infos = r.sbuf, r.gathered, r.infos
    for e in range(experts):
        sbuf[e] = picked[e * pad : e * pad + cap]
    arrivals, notes = {}, []
    for i, hop in enumerate(order):
        if hop:
            to = lax.rem(sp + hop, ns)
            arrivals[i] = send(sbuf.at[to], gathered.at[tp, i], r.sp_sem, (i - 1,), {"sp": to})
    for i, hop in enumerate(order):
        if hop:
            to = lax.rem(sp + hop, ns)
            notes.append(
                send(r.info.at[to], infos.at[i], r.info_sem, (i - 1,), {"sp": to})
            )
    gathered[tp, 0] = sbuf[sp]
    infos[0] = r.info[sp]

    def stats_start(index, summed):
        r.stat_own[index] = row_stats(summed)
        return [
            send(
                r.stat_own.at[index],
                r.stat_in.at[index, hop - 1],
                r.stat_sem,
                (index, hop - 1),
                {"tp": lax.rem(tp + hop, nt)},
            )
            for hop in range(1, nt)
        ]

    def stats_end(index, copies, summed, gain):
        total = r.stat_own[index]
        for hop in range(1, nt):
            copies[hop - 1].wait_recv()
            total = total + r.stat_in[index, hop - 1]
        total = columns_of(total / (width * nt))
        mean, square = total[:, 0:1], total[:, 1:2]
        return (summed - mean) * lax.rsqrt(square - mean * mean + 1e-05) * gain

    first_stats = stats_start(0, projected)
    half = ns // 2
    across, forward = {}, {}

    def arrive(c):
        for i in range(c * half, (c + 1) * half):
            if i:
                arrivals[i].wait_recv()
            mine = gathered.at[tp, i]
            for k in range(1, chips):
                across[i, k] = send(
                    mine, mine, r.y_sem, (i, k - 1),
                    {"tp": 2 * lax.rem(chip + k, chips) + core},
                )
            forward[i, 0] = send(mine, mine, r.pair_sem, (i, 0), {"tp": partner})

    def relay(c):
        for i in range(c * half, (c + 1) * half):
            for k in range(1, chips):
                across[i, k].wait_recv()
                theirs = gathered.at[2 * lax.rem(chip - k + chips, chips) + core, i]
                forward[i, k] = send(theirs, theirs, r.pair_sem, (i, k), {"tp": partner})

    def assemble(c):
        for i in range(c * half, (c + 1) * half):
            for k in range(chips):
                forward[i, k].wait_recv()
            if i:
                notes[i - 1].wait_recv()
            r.side[i * pad : (i + 1) * pad] = columns_of(infos[i])[:pad]
            blocks = [gathered[t, i].astype(F32) for t in range(nt)]
            total = functools.reduce(jnp.add, blocks)
            mean = jnp.sum(total, 1, keepdims=True) / (width * nt)
            blocks = [one - mean for one in blocks]
            square = functools.reduce(jnp.add, [one * one for one in blocks])
            scale = lax.rsqrt(jnp.sum(square, 1, keepdims=True) / (width * nt) + 1e-05)
            for t in range(nt):
                r.inputs[i * pad : i * pad + cap, t * width : (t + 1) * width] = (
                    blocks[t] * scale * gain_in[t][0:1]
                ).astype(BF16)

    tile = 256 if units % 256 == 0 else 128
    silu = jax.nn.silu

    def expert(c):
        rows_here = slice(c * half * pad, (c + 1) * half * pad)
        inputs = r.inputs
        weight_e, shared_e = r.side[rows_here, 0:1], r.side[rows_here, 1:2]
        if joint:
            both = dot(inputs[rows_here], r.cvr[...])
            gate, up = both[:, :narrow], both[:, narrow:]
        else:
            gate = dot(inputs[rows_here], r.cvr[0])
            up = dot(inputs[rows_here], r.cvr[1])
        r.hidden[rows_here, units:] = (silu(gate) * up * shared_e).astype(BF16)

        @pl.loop(0, units // tile)
        def _(i):
            cols = pl.ds(pl.multiple_of(i * tile, tile), tile)
            gate = dot(inputs[rows_here], r.wv[:, cols])
            up = dot(inputs[rows_here], r.wr[:, cols])
            r.hidden[rows_here, cols] = (silu(gate) * up * weight_e).astype(BF16)

    def part_block(c, t):
        rows_here = slice(c * half * pad, (c + 1) * half * pad)
        cols = pl.ds(pl.multiple_of(t * width, width), width)
        return dot(r.hidden[rows_here], hid_w[:, cols])

    part_pairs, part_across, backs = {}, {}, {}

    def lower(c):
        for k in far_first:
            value = part_block(c, 2 * lax.rem(chip + k, chips) + 1 - core).astype(BF16)
            for j in range(half):
                r.part_out[c, k, j] = value[j * pad : j * pad + cap]
            part_pairs[k] = send(
                r.part_out.at[c, k], r.part_in.at[c, k], r.part_sem, (c, k),
                {"tp": partner},
            )
        for k in far_first:
            there = 2 * lax.rem(chip + k, chips) + core
            value = part_block(c, there)
            part_pairs[k].wait_recv()
            for j in range(half):
                piece = value[j * pad : j * pad + cap] + r.part_in[c, k, j].astype(F32)
                if k:
                    r.part_yout[c, k - 1, j] = piece.astype(BF16)
                else:
                    r.own[c, j] = piece
            if k:
                part_across[c, k] = send(
                    r.part_yout.at[c, k - 1], r.part_yin.at[c, k - 1], r.part_sem,
                    (c, chips + k - 1), {"tp": there},
                )

    def give_back(c):
        for k in range(1, chips):
            part_across[c, k].wait_recv()
        for j in range(half):
            i = c * half + j
            piece = r.own[c, j]
            for k in range(1, chips):
                piece = piece + r.part_yin[c, k - 1, j].astype(F32)
            r.back_out[i] = piece.astype(BF16)
            if i:
                to = lax.rem(sp - order[i] + ns, ns)
                backs[i] = send(
                    r.back_out.at[i], r.back_in.at[sp], r.back_sem, (i - 1,), {"sp": to}
                )
            else:
                r.back_in[sp] = r.back_out[0]

    arrive(0)
    arrive(1)
    middle = stats_end(0, first_stats, projected, r.gain[...]).astype(BF16)
    for copy in gain_copies:
        copy.wait_recv()
    relay(0)
    for load in loads[1:5]:
        load.wait()
    assemble(0)
    expert(0)
    relay(1)
    for load in loads[5:]:
        load.wait()
    lower(0)
    assemble(1)
    expert(1)
    give_back(0)
    lower(1)
    give_back(1)
    for i in backs:
        backs[i].wait_recv()
    for j in range(ns):
        r.returned[j * pad : j * pad + cap] = r.back_in[j]
    second = ALPHA * middle.astype(F32) + dot(r.pick_t[...], r.returned[...])
    copies = stats_start(1, second)
    out_ref[...] = stats_end(1, copies, second, r.last_gain[...]).astype(out_ref.dtype)
    if groups_all > 1:
        for index, hop in enumerate(hops):

            @pl.when(group + hop < groups_all)
            def _():
                scan_copy(index).wait_send()

        note.wait_send()
    for copy in waits:
        copy.wait_send()


def shards(
    probe_vectors,
    address_vectors,
    content_vectors,
    storage_raw_signal,
    fade_raw_signal,
    channel_fade_exponent,
    extra_fade_amount,
    sequence_label,
    exit_valve_raw_signal,
    final_projection_matrix,
    incoming_rows_matrix,
    initial_rescale_factor,
    specialist_picks,
    picked_specialist_share,
    specialist_valve_matrix,
    specialist_raising_matrix,
    specialist_lowering_matrix,
    common_valve_matrix,
    common_raising_matrix,
    common_lowering_matrix,
    latter_rescale_factor,
):
    ns, nt = lax.axis_size("sp"), lax.axis_size("tp")
    tokens, width = incoming_rows_matrix.shape
    heads = storage_raw_signal.shape[0]
    experts = specialist_valve_matrix.shape[0] * ns
    top = specialist_picks.shape[1]
    cap = max(2, 9 * tokens * top // (8 * experts))
    pad = -(-cap // 16) * 16
    size = GROUP
    while heads % size or ns % size:
        size //= 2
    held = heads // size
    reach = -(-(DOC_SPAN - 1) // tokens)
    hops = scan_plan(ns // size, -(-reach // size))
    rounds = len(hops)
    units, narrow = specialist_valve_matrix.shape[2], common_valve_matrix.shape[1]
    features = width * nt
    chips = nt // 2
    across = max(chips - 1, 1)
    half = ns // 2
    swap = max(size - 1, 1)
    dma = pltpu.SemaphoreType.DMA

    def vm(*shape, dtype=BF16):
        return pltpu.VMEM(shape, dtype)

    f32 = functools.partial(vm, dtype=F32)
    operands = dict(
        queries=probe_vectors,
        keys=address_vectors,
        values=content_vectors,
        gate=exit_valve_raw_signal,
        storage=storage_raw_signal,
        fade=fade_raw_signal,
        fade_exp=channel_fade_exponent[None, :],
        extra=extra_fade_amount,
        label=sequence_label[None, :],
        rows=incoming_rows_matrix,
        gain=initial_rescale_factor[None, :],
        last_gain=latter_rescale_factor[None, :],
        picks=specialist_picks,
        share=picked_specialist_share,
    )
    weights = dict(
        wo_hbm=final_projection_matrix,
        wv_hbm=specialist_valve_matrix,
        wr_hbm=specialist_raising_matrix,
        wd_hbm=specialist_lowering_matrix,
        cv_hbm=common_valve_matrix,
        cr_hbm=common_raising_matrix,
        cd_hbm=common_lowering_matrix,
    )
    scratch = dict(
        wo=vm(*final_projection_matrix.shape),
        wv=vm(features, units),
        wr=vm(features, units),
        cvr=vm(features, 2 * narrow) if narrow % 128 == 0 else vm(2, features, narrow),
        wd=vm(units + narrow, features),
        weight_sem=dma((7,)),
        scal_out=f32(heads, 8, tokens),
        scal_in=f32(size, held, 8, tokens),
        keys_in=vm(size, tokens, held * DK),
        values_in=vm(size, tokens, held * DV),
        queries_in=vm(size, tokens, held * DK),
        gate_in=vm(size, tokens, held * DV),
        swap_sem=dma((2, 5, swap)),
        gain_out=f32(8, width),
        gain_in=f32(nt, 8, width),
        gain_sem=dma((2, nt - 1)),
        pick=vm(experts * pad, tokens),
        pick_t=vm(tokens, experts * pad),
        info=f32(experts, 8, 128),
        infos=f32(ns, 8, 128),
        info_sem=dma((2, ns - 1)),
        inverse=f32(size, held, tokens, tokens),
        decay=f32(size, held, tokens, tokens),
        norm=f32(size, held, 8, tokens),
        built=vm(rounds, 2, held, DK, DV),
        landed=vm(rounds, 2, held, DK, DV),
        scan_sem=dma((2, rounds)),
        label_note=f32(8, tokens),
        note_sem=dma((2,)),
        reader=vm(held, size * tokens, DK),
        partial=f32(held, size * tokens, DV),
        mixed=vm(size, tokens, held * DV),
        heads=vm(tokens, heads * DV),
        give_sem=dma((2, swap)),
        head_out=vm(chips, tokens, width),
        head_in=vm(chips, tokens, width),
        head_yout=vm(across, tokens, width),
        head_yin=vm(across, tokens, width),
        head_sem=dma((2, 2 * chips)),
        stat_own=f32(2, 8, tokens),
        stat_in=f32(2, nt - 1, 8, tokens),
        stat_sem=dma((2, 2, nt - 1)),
        sbuf=vm(ns, cap, width),
        gathered=vm(nt, ns, cap, width),
        sp_sem=dma((2, ns - 1)),
        y_sem=dma((2, ns, across)),
        pair_sem=dma((2, ns, chips)),
        inputs=vm(ns * pad, features),
        hidden=vm(ns * pad, units + narrow),
        side=f32(ns * pad, 128),
        part_out=vm(2, chips, half, cap, width),
        part_in=vm(2, chips, half, cap, width),
        part_yout=vm(2, across, half, cap, width),
        part_yin=vm(2, across, half, cap, width),
        part_sem=dma((2, 2, 2 * chips)),
        own=f32(2, half, cap, width),
        back_out=vm(ns, cap, width),
        back_in=vm(ns, cap, width),
        back_sem=dma((2, ns - 1)),
        returned=vm(ns * pad, width),
    )
    plan = SimpleNamespace(
        names=tuple(operands) + tuple(weights) + ("out",) + tuple(scratch),
        ns=ns,
        nt=nt,
        cap=cap,
        pad=pad,
        size=size,
        held=held,
        hops=hops,
    )
    return pl.pallas_call(
        functools.partial(whole_kernel, plan),
        out_shape=jax.ShapeDtypeStruct((tokens, width), BF16),
        in_specs=[pl.BlockSpec(memory_space=pltpu.VMEM)] * len(operands)
        + [pl.BlockSpec(memory_space=pl.ANY)] * len(weights),
        out_specs=pl.BlockSpec(memory_space=pltpu.VMEM),
        scratch_shapes=list(scratch.values()),
        compiler_params=pltpu.CompilerParams(
            collective_id=1, has_side_effects=True, vmem_limit_bytes=60 * 2**20
        ),
        name="whole_layer",
    )(*operands.values(), *weights.values())


def solution(mesh):
    placed = (
        P("sp", "tp"),
        P("sp", "tp"),
        P("sp", "tp"),
        P("tp", "sp"),
        P("tp", "sp"),
        P("tp"),
        P("tp", "sp"),
        P("sp"),
        P("sp", "tp"),
        P("tp", None),
        P("sp", "tp"),
        P("tp"),
        P("sp", None),
        P("sp", None),
        P("sp", None, "tp"),
        P("sp", None, "tp"),
        P("sp", "tp", None),
        P(None, "tp"),
        P(None, "tp"),
        P("tp", None),
        P("tp"),
    )
    return jax.shard_map(
        shards, mesh=mesh, in_specs=placed, out_specs=P("sp", "tp"), check_vma=False
    )
```

time: 110 us -> 75 us (0.68)
  Pallas kernels: 85.8 us -> 70.5 us
  other arithmetic: 9.26 us -> 0 us
  matrix products: 7.11 us -> 0 us
  local copies, waits for them, and re-layouts: 7.01 us -> 4.35 us
    pallas_call x2 -> x1, Pallas kernels: 85.8 us -> 70.5 us  [shards(): pl.pallas_call(functools.partial(whole_kernel, plan), out_shape=jax.Shape...]
    dot_general x23 -> x0, matrix products: 7.11 us -> none  [the longest x12 4.03 us: matmul_one(): jnp.einsum(form, left.astype(jnp.bfloat16), right.astype(jnp.bfloat16), p...]
    convert_element_type x9 -> x0, other arithmetic: 3.64 us -> none  [the longest x1 1.41 us: block_pass(): (segment[:, -1] == before).astype(jnp.float32)]
    another operation x4 -> x0, other arithmetic: 2.4 us -> none  [the longest x1 0.95 us: block_pass(): cumulative = jnp.cumsum(decay_logarithm, -1)]
    unnamed x14 -> x3, local copies, waits for them, and re-layouts: 2.85 us -> 4.35 us
    slice x5 -> x0, local copies, waits for them, and re-layouts: 1.23 us -> none  [the longest x1 0.66 us: block_pass(): before = jnp.concatenate([segment[:1, 0], segment[:-1, -1]])]
where the time goes in v1:
time: 75 us; the launch traced here: 74.9 us
  Pallas kernels  70.5 us (94%)
  local copies, waits for them, and re-layouts  4.35 us (6%)
    pallas_call x1, Pallas kernels, shards(): pl.pallas_call(functools.partial(whole_kernel, plan), out_shape=jax.Shape...  70.5 us
    unnamed x3, local copies, waits for them, and re-layouts  4.35 us

profile of v1, /device:TPU:0, one launch (start us, length us, event | category | flops | bytes accessed | tf_op | source)
XLA Modules:
  0.0 74.9 jit_solution(4864635680083957570)
XLA Ops:
  0.0 1.4 %copy.23.refs_13_ = bf16[128,2]{1,0:T(8,128)(2,1)} copy(bf16[128,2]{0,1:T(2,128)(2,1)} %param.34) | data formatting | bytes 1024 | tf_op args[13]
  1.4 1.4 %copy.22.refs_12_ = s32[128,2]{1,0:T(8,128)} copy(s32[128,2]{0,1:T(2,128)} %param.33) | data formatting | bytes 2048 | tf_op args[12]
  2.8 70.5 %whole_layer.1 = bf16[128,512]{1,0:T(8,128)(2,1)} custom-call(bf16[128,512]{1,0:T(8,128)(2,1)} %refs_0_.1, bf16[128,512]{1,0:T(8,128)(2,1)} %refs_1_.1, bf16[128,512]{1,0:T(8,128)(2,1)} %refs_2_.1, bf16[128,512]{1,0:T(8,128)(2,1)} %refs_3_.1, f32[4,128]{1,0:T(4,128)} %refs_4_.1, f32[4,128]{1,0:T(4,128)} %refs_5_.1, f32[1,4]{1,0:T(1,128)} %bitcast.6, ...), custom_call_target="tpu_custom_call" | custom-call | tf_op jit(solution)/shard_map/whole_layer/pallas_call | solution.py:799
  73.3 1.6 %copy.25 = bf16[128,512]{1,0:T(8,128)(2,1)} copy(bf16[128,512]{1,0:T(8,128)(2,1)} %whole_layer.1) | data formatting | bytes 262144

commit v2 on v1

--- a/solution.py
+++ b/solution.py
@@ -70,7 +70,7 @@
     r = SimpleNamespace(**dict(zip(plan.names, refs)))
     ns, nt, cap, pad = plan.ns, plan.nt, plan.cap, plan.pad
     size, held, hops = plan.size, plan.held, plan.hops
-    order = hop_order(ns)
+    order, bounds = hop_order(ns), plan.bounds
     groups_all = ns // size
     sp, tp = lax.axis_index("sp"), lax.axis_index("tp")
     chips = nt // 2
@@ -104,6 +104,18 @@
         pltpu.make_async_copy(source, target, r.weight_sem.at[i])
         for i, (source, target) in enumerate(pairs)
     ]
+    takes = {
+        name: pltpu.make_async_copy(
+            getattr(r, name + "_hbm"), getattr(r, name), r.take_sem.at[i]
+        )
+        for i, name in enumerate(plan.inputs)
+    }
+    for take in takes.values():
+        take.start()
+
+    def have(*names):
+        for name in names or tuple(takes):
+            takes.pop(name).wait()
     barrier = pltpu.get_barrier_semaphore()
     for hop in range(1, ns):
         pl.semaphore_signal(
@@ -113,11 +125,9 @@
         pl.semaphore_signal(
             barrier, inc=1, device_id={"tp": lax.rem(tp + hop, nt)}, device_id_type=MESH
         )
-    for load in loads:
-        load.start()
-
     row, col = iota((tokens, tokens), 0), iota((tokens, tokens), 1)
     upper = (row <= col).astype(BF16)
+    have("fade_exp", "extra", "fade", "storage", "label", "gain")
     rate = jnp.exp(r.fade_exp[...])
     eye_h = iota((heads, heads), 0) == iota((heads, heads), 1)
     rate = jnp.sum(jnp.where(eye_h, rate, 0.0), 1, keepdims=True)
@@ -137,6 +147,7 @@
         scal_out[h] = jnp.where(slot == 2, label, tile)
     r.gain_out[...] = jnp.broadcast_to(r.gain[...], r.gain_out.shape)
     pl.semaphore_wait(barrier, ns - 1 + nt - 1)
+    have()
     waits = []
 
     def send(source, target, sems, place, where):
@@ -179,12 +190,18 @@
     for name in ("keys", "values", "queries", "gate"):
         getattr(r, name + "_in")[member] = part_of(getattr(r, name), member)[...]
 
+    for load in loads:
+        load.start()
     r.inputs[...] = jnp.zeros_like(r.inputs)
     r.returned[...] = jnp.zeros_like(r.returned)
 
-    pick_a = r.picks[:, 0:1].astype(F32)
-    pick_b = r.picks[:, 1:2].astype(F32)
-    share = r.share[...].astype(F32)
+    pick_rows, share_rows = r.picks[...].astype(F32), r.share[...].astype(F32)
+    fact_rows = jnp.where(slot == 0, pick_rows[0:1], 0.0)
+    fact_rows = jnp.where(slot == 1, share_rows[0:1], fact_rows)
+    fact_rows = jnp.where(slot == 2, share_rows[1:2], fact_rows)
+    fact_rows = jnp.where(slot == 3, 1.0, fact_rows)
+    pick_cols = columns_of(jnp.where(slot == 4, pick_rows[1:2], fact_rows))
+    pick_a, pick_b = pick_cols[:, 0:1], pick_cols[:, 4:5]
     lane = iota((tokens, 128), 1)
     lane_f = lane.astype(F32)
     member_of = ((pick_a == lane_f) | (pick_b == lane_f)).astype(F32)
@@ -201,11 +218,7 @@
     pick_t = (dot(coded, spread) == local[0:1]).astype(F32)
     r.pick_t[...] = pick_t.astype(BF16)
     r.pick[...] = pick_t.T.astype(BF16)
-    facts = jnp.where(lane == 0, pick_a, 0.0)
-    facts = jnp.where(lane == 1, share[:, 0:1], facts)
-    facts = jnp.where(lane == 2, share[:, 1:2], facts)
-    facts = jnp.where(lane == 3, 1.0, facts).T[:8].astype(BF16)
-    facts = dot(facts, pick_t.astype(BF16))
+    facts = dot(fact_rows.astype(BF16), pick_t.astype(BF16))
     leads = facts[0:1] == expert_of[0:1]
     slot_weight = jnp.where(leads, facts[1:2], facts[2:3])
     slot_shared = jnp.where(leads, facts[3:4], 0.0)
@@ -213,6 +226,13 @@
     r.info[...] = jnp.zeros_like(r.info)
     for e in range(experts):
         r.info[e, :, 0:pad] = side_rows[:, e * pad : (e + 1) * pad]
+
+    infos, notes = r.infos, {}
+    for i, hop in enumerate(order):
+        if hop:
+            to = lax.rem(sp + hop, ns)
+            notes[i] = send(r.info.at[to], infos.at[i], r.info_sem, (i,), {"sp": to})
+    infos[0] = r.info[sp]
 
     same = row == col
     inverse_ref, decay_ref, norm_ref = r.inverse, r.decay, r.norm
@@ -461,22 +481,15 @@
         projected = projected + r.head_yin[k].astype(F32)
 
     picked = dot(r.pick[...], projected.astype(BF16)).astype(BF16)
-    sbuf, gathered, infos = r.sbuf, r.gathered, r.infos
+    sbuf, gathered = r.sbuf, r.gathered
     for e in range(experts):
         sbuf[e] = picked[e * pad : e * pad + cap]
-    arrivals, notes = {}, []
+    arrivals = {}
     for i, hop in enumerate(order):
         if hop:
             to = lax.rem(sp + hop, ns)
-            arrivals[i] = send(sbuf.at[to], gathered.at[tp, i], r.sp_sem, (i - 1,), {"sp": to})
-    for i, hop in enumerate(order):
-        if hop:
-            to = lax.rem(sp + hop, ns)
-            notes.append(
-                send(r.info.at[to], infos.at[i], r.info_sem, (i - 1,), {"sp": to})
-            )
+            arrivals[i] = send(sbuf.at[to], gathered.at[tp, i], r.sp_sem, (i,), {"sp": to})
     gathered[tp, 0] = sbuf[sp]
-    infos[0] = r.info[sp]
 
     def stats_start(index, summed):
         r.stat_own[index] = row_stats(summed)
@@ -500,13 +513,11 @@
         mean, square = total[:, 0:1], total[:, 1:2]
         return (summed - mean) * lax.rsqrt(square - mean * mean + 1e-05) * gain
 
-    first_stats = stats_start(0, projected)
-    half = ns // 2
     across, forward = {}, {}
 
     def arrive(c):
-        for i in range(c * half, (c + 1) * half):
-            if i:
+        for i in range(bounds[c], bounds[c + 1]):
+            if order[i]:
                 arrivals[i].wait_recv()
             mine = gathered.at[tp, i]
             for k in range(1, chips):
@@ -517,18 +528,18 @@
             forward[i, 0] = send(mine, mine, r.pair_sem, (i, 0), {"tp": partner})
 
     def relay(c):
-        for i in range(c * half, (c + 1) * half):
+        for i in range(bounds[c], bounds[c + 1]):
             for k in range(1, chips):
                 across[i, k].wait_recv()
                 theirs = gathered.at[2 * lax.rem(chip - k + chips, chips) + core, i]
                 forward[i, k] = send(theirs, theirs, r.pair_sem, (i, k), {"tp": partner})
 
     def assemble(c):
-        for i in range(c * half, (c + 1) * half):
+        for i in range(bounds[c], bounds[c + 1]):
             for k in range(chips):
                 forward[i, k].wait_recv()
-            if i:
-                notes[i - 1].wait_recv()
+            if order[i]:
+                notes[i].wait_recv()
             r.side[i * pad : (i + 1) * pad] = columns_of(infos[i])[:pad]
             blocks = [gathered[t, i].astype(F32) for t in range(nt)]
             total = functools.reduce(jnp.add, blocks)
@@ -545,7 +556,7 @@
     silu = jax.nn.silu
 
     def expert(c):
-        rows_here = slice(c * half * pad, (c + 1) * half * pad)
+        rows_here = slice(bounds[c] * pad, bounds[c + 1] * pad)
         inputs = r.inputs
         weight_e, shared_e = r.side[rows_here, 0:1], r.side[rows_here, 1:2]
         if joint:
@@ -564,73 +575,75 @@
             r.hidden[rows_here, cols] = (silu(gate) * up * weight_e).astype(BF16)
 
     def part_block(c, t):
-        rows_here = slice(c * half * pad, (c + 1) * half * pad)
+        rows_here = slice(bounds[c] * pad, bounds[c + 1] * pad)
         cols = pl.ds(pl.multiple_of(t * width, width), width)
         return dot(r.hidden[rows_here], hid_w[:, cols])
 
     part_pairs, part_across, backs = {}, {}, {}
 
     def lower(c):
+        low, top = bounds[c], bounds[c + 1]
         for k in far_first:
             value = part_block(c, 2 * lax.rem(chip + k, chips) + 1 - core).astype(BF16)
-            for j in range(half):
-                r.part_out[c, k, j] = value[j * pad : j * pad + cap]
+            for i in range(low, top):
+                r.part_out[k, i] = value[(i - low) * pad : (i - low) * pad + cap]
             part_pairs[k] = send(
-                r.part_out.at[c, k], r.part_in.at[c, k], r.part_sem, (c, k),
+                r.part_out.at[k, low:top], r.part_in.at[k, low:top], r.part_sem, (c, k),
                 {"tp": partner},
             )
         for k in far_first:
             there = 2 * lax.rem(chip + k, chips) + core
             value = part_block(c, there)
             part_pairs[k].wait_recv()
-            for j in range(half):
-                piece = value[j * pad : j * pad + cap] + r.part_in[c, k, j].astype(F32)
+            for i in reversed(range(low, top)):
+                piece = value[(i - low) * pad : (i - low) * pad + cap]
+                piece = piece + r.part_in[k, i].astype(F32)
                 if k:
-                    r.part_yout[c, k - 1, j] = piece.astype(BF16)
+                    r.part_yout[k - 1, i] = piece.astype(BF16)
+                    part_across[k, i] = send(
+                        r.part_yout.at[k - 1, i], r.part_yin.at[k - 1, i], r.fold_sem,
+                        (i, k - 1), {"tp": there},
+                    )
                 else:
-                    r.own[c, j] = piece
-            if k:
-                part_across[c, k] = send(
-                    r.part_yout.at[c, k - 1], r.part_yin.at[c, k - 1], r.part_sem,
-                    (c, chips + k - 1), {"tp": there},
-                )
+                    r.own[i] = piece
 
     def give_back(c):
-        for k in range(1, chips):
-            part_across[c, k].wait_recv()
-        for j in range(half):
-            i = c * half + j
-            piece = r.own[c, j]
+        for i in reversed(range(bounds[c], bounds[c + 1])):
+            piece = r.own[i]
             for k in range(1, chips):
-                piece = piece + r.part_yin[c, k - 1, j].astype(F32)
+                part_across[k, i].wait_recv()
+                piece = piece + r.part_yin[k - 1, i].astype(F32)
             r.back_out[i] = piece.astype(BF16)
-            if i:
+            if order[i]:
                 to = lax.rem(sp - order[i] + ns, ns)
                 backs[i] = send(
-                    r.back_out.at[i], r.back_in.at[sp], r.back_sem, (i - 1,), {"sp": to}
+                    r.back_out.at[i], r.back_in.at[sp], r.back_sem, (i,), {"sp": to}
                 )
             else:
-                r.back_in[sp] = r.back_out[0]
-
-    arrive(0)
-    arrive(1)
-    middle = stats_end(0, first_stats, projected, r.gain[...]).astype(BF16)
+                r.back_in[sp] = r.back_out[i]
+
+    chunks = len(bounds) - 1
+    for c in range(chunks):
+        arrive(c)
+    relay(0)
+    first_stats = stats_start(0, projected)
     for copy in gain_copies:
         copy.wait_recv()
-    relay(0)
     for load in loads[1:5]:
         load.wait()
-    assemble(0)
-    expert(0)
-    relay(1)
-    for load in loads[5:]:
-        load.wait()
-    lower(0)
-    assemble(1)
-    expert(1)
-    give_back(0)
-    lower(1)
-    give_back(1)
+    for c in range(chunks):
+        assemble(c)
+        expert(c)
+        if c + 1 < chunks:
+            relay(c + 1)
+        if c:
+            give_back(c - 1)
+        else:
+            for load in loads[5:]:
+                load.wait()
+        lower(c)
+    give_back(chunks - 1)
+    middle = stats_end(0, first_stats, projected, r.gain[...]).astype(BF16)
     for i in backs:
         backs[i].wait_recv()
     for j in range(ns):
@@ -691,7 +704,7 @@
     features = width * nt
     chips = nt // 2
     across = max(chips - 1, 1)
-    half = ns // 2
+    bounds = (0, 3 * ns // 8, ns)
     swap = max(size - 1, 1)
     dma = pltpu.SemaphoreType.DMA
 
@@ -700,20 +713,20 @@
 
     f32 = functools.partial(vm, dtype=F32)
     operands = dict(
-        queries=probe_vectors,
-        keys=address_vectors,
-        values=content_vectors,
-        gate=exit_valve_raw_signal,
         storage=storage_raw_signal,
         fade=fade_raw_signal,
         fade_exp=channel_fade_exponent[None, :],
         extra=extra_fade_amount,
         label=sequence_label[None, :],
+        keys=address_vectors,
+        values=content_vectors,
+        queries=probe_vectors,
+        gate=exit_valve_raw_signal,
         rows=incoming_rows_matrix,
         gain=initial_rescale_factor[None, :],
         last_gain=latter_rescale_factor[None, :],
-        picks=specialist_picks,
-        share=picked_specialist_share,
+        picks=specialist_picks.T,
+        share=picked_specialist_share.T,
     )
     weights = dict(
         wo_hbm=final_projection_matrix,
@@ -724,7 +737,10 @@
         cr_hbm=common_raising_matrix,
         cd_hbm=common_lowering_matrix,
     )
+    shapes = {name: pltpu.VMEM(one.shape, one.dtype) for name, one in operands.items()}
     scratch = dict(
+        **shapes,
+        take_sem=dma((len(operands),)),
         wo=vm(*final_projection_matrix.shape),
         wv=vm(features, units),
         wr=vm(features, units),
@@ -745,7 +761,7 @@
         pick_t=vm(tokens, experts * pad),
         info=f32(experts, 8, 128),
         infos=f32(ns, 8, 128),
-        info_sem=dma((2, ns - 1)),
+        info_sem=dma((2, ns)),
         inverse=f32(size, held, tokens, tokens),
         decay=f32(size, held, tokens, tokens),
         norm=f32(size, held, 8, tokens),
@@ -769,29 +785,32 @@
         stat_sem=dma((2, 2, nt - 1)),
         sbuf=vm(ns, cap, width),
         gathered=vm(nt, ns, cap, width),
-        sp_sem=dma((2, ns - 1)),
+        sp_sem=dma((2, ns)),
         y_sem=dma((2, ns, across)),
         pair_sem=dma((2, ns, chips)),
         inputs=vm(ns * pad, features),
         hidden=vm(ns * pad, units + narrow),
         side=f32(ns * pad, 128),
-        part_out=vm(2, chips, half, cap, width),
-        part_in=vm(2, chips, half, cap, width),
-        part_yout=vm(2, across, half, cap, width),
-        part_yin=vm(2, across, half, cap, width),
-        part_sem=dma((2, 2, 2 * chips)),
-        own=f32(2, half, cap, width),
+        part_out=vm(chips, ns, cap, width),
+        part_in=vm(chips, ns, cap, width),
+        part_yout=vm(across, ns, cap, width),
+        part_yin=vm(across, ns, cap, width),
+        part_sem=dma((2, len(bounds) - 1, chips)),
+        fold_sem=dma((2, ns, across)),
+        own=f32(ns, cap, width),
         back_out=vm(ns, cap, width),
         back_in=vm(ns, cap, width),
-        back_sem=dma((2, ns - 1)),
+        back_sem=dma((2, ns)),
         returned=vm(ns * pad, width),
     )
     plan = SimpleNamespace(
-        names=tuple(operands) + tuple(weights) + ("out",) + tuple(scratch),
+        names=tuple(name + "_hbm" for name in operands) + tuple(weights) + ("out",) + tuple(scratch),
+        inputs=tuple(operands),
         ns=ns,
         nt=nt,
         cap=cap,
         pad=pad,
+        bounds=bounds,
         size=size,
         held=held,
         hops=hops,
@@ -799,8 +818,7 @@
     return pl.pallas_call(
         functools.partial(whole_kernel, plan),
         out_shape=jax.ShapeDtypeStruct((tokens, width), BF16),
-        in_specs=[pl.BlockSpec(memory_space=pltpu.VMEM)] * len(operands)
-        + [pl.BlockSpec(memory_space=pl.ANY)] * len(weights),
+        in_specs=[pl.BlockSpec(memory_space=pl.ANY)] * (len(operands) + len(weights)),
         out_specs=pl.BlockSpec(memory_space=pltpu.VMEM),
         scratch_shapes=list(scratch.values()),
         compiler_params=pltpu.CompilerParams(

time: 75 us -> 66.7 us (0.89)
  Pallas kernels: 70.5 us -> 65 us
  local copies, waits for them, and re-layouts: 4.35 us -> 1.57 us
    pallas_call x1, Pallas kernels: 70.5 us -> 65 us  [shards(): pl.pallas_call(functools.partial(whole_kernel, plan), out_shape=jax.Shape...]
    unnamed x3 -> x1, local copies, waits for them, and re-layouts: 4.35 us -> 1.57 us
where the time goes in v2:
time: 66.7 us; the launch traced here: 66.5 us
  Pallas kernels  65 us (97%)
  local copies, waits for them, and re-layouts  1.57 us (2%)
    pallas_call x1, Pallas kernels, shards(): pl.pallas_call(functools.partial(whole_kernel, plan), out_shape=jax.Shape...  65 us
    unnamed x1, local copies, waits for them, and re-layouts  1.57 us

profile of v2, /device:TPU:0, one launch (start us, length us, event | category | flops | bytes accessed | tf_op | source)
XLA Modules:
  0.0 66.5 jit_solution(9830405566181189254)
XLA Ops:
  0.0 65.0 %whole_layer.1 = bf16[128,512]{1,0:T(8,128)(2,1)} custom-call(f32[4,128]{1,0:T(4,128)} %refs_0_.1, f32[4,128]{1,0:T(4,128)} %refs_1_.1, f32[1,4]{1,0:T(1,128)} %bitcast.9, f32[4,128]{1,0:T(4,128)} %refs_3_.1, s32[1,128]{1,0:T(1,128)} %bitcast.10, bf16[128,512]{1,0:T(8,128)(2,1)} %refs_5_.1, bf16[128,512]{1,0:T(8,128)(2,1)} %refs_6_.1, ...), custom_call_target="tpu_custom_call" | custom-call | tf_op jit(solution)/shard_map/whole_layer/pallas_call | solution.py:818
  65.0 1.6 %copy.23 = bf16[128,512]{1,0:T(8,128)(2,1)} copy(bf16[128,512]{1,0:T(8,128)(2,1)} %whole_layer.1) | data formatting | bytes 262144

commit v3 on v2

--- a/solution.py
+++ b/solution.py
@@ -36,7 +36,7 @@
         order.append(near)
         if n - near != near:
             order.append(n - near)
-    return order
+    return sorted(order, key=lambda hop: hop % 2)
 
 
 def dot(left, right):
@@ -555,7 +555,7 @@
     tile = 256 if units % 256 == 0 else 128
     silu = jax.nn.silu
 
-    def expert(c):
+    def expert(c, after=None):
         rows_here = slice(bounds[c] * pad, bounds[c + 1] * pad)
         inputs = r.inputs
         weight_e, shared_e = r.side[rows_here, 0:1], r.side[rows_here, 1:2]
@@ -567,12 +567,13 @@
             up = dot(inputs[rows_here], r.cvr[1])
         r.hidden[rows_here, units:] = (silu(gate) * up * shared_e).astype(BF16)
 
-        @pl.loop(0, units // tile)
-        def _(i):
-            cols = pl.ds(pl.multiple_of(i * tile, tile), tile)
+        for i in range(units // tile):
+            cols = slice(i * tile, (i + 1) * tile)
             gate = dot(inputs[rows_here], r.wv[:, cols])
             up = dot(inputs[rows_here], r.wr[:, cols])
             r.hidden[rows_here, cols] = (silu(gate) * up * weight_e).astype(BF16)
+            if after is not None and i == (units // tile - 1) // 2:
+                after(c - 1)
 
     def part_block(c, t):
         rows_here = slice(bounds[c] * pad, bounds[c + 1] * pad)
@@ -581,20 +582,23 @@
 
     part_pairs, part_across, backs = {}, {}, {}
 
-    def lower(c):
+    def lower_pairs(c):
         low, top = bounds[c], bounds[c + 1]
         for k in far_first:
             value = part_block(c, 2 * lax.rem(chip + k, chips) + 1 - core).astype(BF16)
             for i in range(low, top):
                 r.part_out[k, i] = value[(i - low) * pad : (i - low) * pad + cap]
-            part_pairs[k] = send(
+            part_pairs[c, k] = send(
                 r.part_out.at[k, low:top], r.part_in.at[k, low:top], r.part_sem, (c, k),
                 {"tp": partner},
             )
+
+    def lower_own(c):
+        low, top = bounds[c], bounds[c + 1]
         for k in far_first:
             there = 2 * lax.rem(chip + k, chips) + core
             value = part_block(c, there)
-            part_pairs[k].wait_recv()
+            part_pairs[c, k].wait_recv()
             for i in reversed(range(low, top)):
                 piece = value[(i - low) * pad : (i - low) * pad + cap]
                 piece = piece + r.part_in[k, i].astype(F32)
@@ -629,19 +633,17 @@
     first_stats = stats_start(0, projected)
     for copy in gain_copies:
         copy.wait_recv()
-    for load in loads[1:5]:
+    for load in loads[1:]:
         load.wait()
     for c in range(chunks):
         assemble(c)
-        expert(c)
+        expert(c, lower_own if c else None)
         if c + 1 < chunks:
             relay(c + 1)
+        lower_pairs(c)
         if c:
             give_back(c - 1)
-        else:
-            for load in loads[5:]:
-                load.wait()
-        lower(c)
+    lower_own(chunks - 1)
     give_back(chunks - 1)
     middle = stats_end(0, first_stats, projected, r.gain[...]).astype(BF16)
     for i in backs:

time: 66.7 us -> 65.3 us (0.979)
  Pallas kernels: 65 us -> 63.6 us
    pallas_call x1, Pallas kernels: 65 us -> 63.6 us  [shards(): pl.pallas_call(functools.partial(whole_kernel, plan), out_shape=jax.Shape...]
where the time goes in v3:
time: 65.3 us; the launch traced here: 65.1 us
  Pallas kernels  63.6 us (97%)
  local copies, waits for them, and re-layouts  1.57 us (2%)
    pallas_call x1, Pallas kernels, shards(): pl.pallas_call(functools.partial(whole_kernel, plan), out_shape=jax.Shape...  63.6 us
    unnamed x1, local copies, waits for them, and re-layouts  1.57 us

profile of v3, /device:TPU:0, one launch (start us, length us, event | category | flops | bytes accessed | tf_op | source)
XLA Modules:
  0.0 65.1 jit_solution(357697138552578075)
XLA Ops:
  0.0 63.6 %whole_layer.1 = bf16[128,512]{1,0:T(8,128)(2,1)} custom-call(f32[4,128]{1,0:T(4,128)} %refs_0_.1, f32[4,128]{1,0:T(4,128)} %refs_1_.1, f32[1,4]{1,0:T(1,128)} %bitcast.9, f32[4,128]{1,0:T(4,128)} %refs_3_.1, s32[1,128]{1,0:T(1,128)} %bitcast.10, bf16[128,512]{1,0:T(8,128)(2,1)} %refs_5_.1, bf16[128,512]{1,0:T(8,128)(2,1)} %refs_6_.1, ...), custom_call_target="tpu_custom_call" | custom-call | tf_op jit(solution)/shard_map/whole_layer/pallas_call | solution.py:820
  63.6 1.6 %copy.23 = bf16[128,512]{1,0:T(8,128)(2,1)} copy(bf16[128,512]{1,0:T(8,128)(2,1)} %whole_layer.1) | data formatting | bytes 262144
